TPU v7x, 256 devices: a whole 4x4x8 slice. The times are simulated.
256 devices in a mesh: ep: 16 (over y, x), tp: 16 (over z, core).
Axes of the slice: x: 4, y: 4, z: 8, core: 2. Of those that a mesh axis runs over, the one named last changes fastest.
Arguments:
- query_preactivation: bfloat16 [32768, 2048], P('ep', 'tp'), may hold values from -6 to 6
- forget_preactivation: bfloat16 [32768, 2048], P('ep', 'tp'), may hold values from -6 to 6
- value_input_rows: bfloat16 [32768, 1024], P('ep', 'tp'), may hold values from -8 to 8
- output_gate_preactivation: bfloat16 [32768, 1024], P('ep', 'tp'), may hold values from -6 to 6
- forget_floor_gap: float32 [2048], P('tp'), may hold values from 0 to 0.2, as said below
- extra_log_forget: float32 [32768, 16], P('ep', 'tp'), may hold values from -2 to 0
- head_output_gain: float32 [1024], P('tp'), may hold values from 0.1 to 1.9
- mixer_output_weight: bfloat16 [1024, 2048], P(None, 'tp'), may hold values from -0.1875 to 0.1875
- second_batch_tokens: bfloat16 [8192, 2048], P('ep'), may hold values from -6 to 6
- feedforward_norm_gain: float32 [2048], replicated, may hold values from 0.1 to 1.9
- chosen_expert_index: int32 [8192, 2], P('ep'), may hold values from 0 to 15, all different within a row; in each aligned block of 32 rows (0 to 31, 32 to 63, ...) at most 5 rows name the same one
- chosen_expert_weight: float32 [8192, 2], P('ep'), may hold values from 0.1 to 1
- expert_gate_weight: bfloat16 [16, 2048, 7168], P('ep', None, 'tp'), may hold values from -0.125 to 0.125
- expert_up_weight: bfloat16 [16, 2048, 7168], P('ep', None, 'tp'), may hold values from -0.125 to 0.125
- expert_down_weight: bfloat16 [16, 7168, 2048], P('ep', 'tp'), may hold values from -0.0625 to 0.0625
Outputs:
- mixer_output_first: bfloat16 [32768, 2048], P('ep', 'tp')
- moe_out: bfloat16 [8192, 2048], P(('ep', 'tp'))
Inputs may be any that keep to these rules, and one draw needn't show every extreme that they name: `chosen_expert_index`: each row names 2 different experts. In each aligned block of 32 rows (the rows of one device's share) no expert is named by more than 5 rows, and in every draw some expert is named by exactly 5 rows of some block. `forget_floor_gap`: every entry is positive.
All inputs are finite; a program needn't handle non-finite values.
Results may differ from a plain program's by a relative error of at most 0.019.
Values may be sent and summed in bfloat16 or wider, within the bound.
A program may use at most 128 MiB of HBM per device.

v0:
```python
import jax
import jax.numpy as jnp
from jax import lax
from jax.sharding import PartitionSpec as P

KEY_DIM = 128
VAL_DIM = 64
BLOCK_POSITIONS = 64
TOPK = 2
epsilon = 1e-06


def copy_for_each(shard, axis):
    copies = jnp.broadcast_to(shard, (lax.axis_size(axis), *shard.shape))
    return lax.all_to_all(copies, axis, split_axis=0, concat_axis=0, tiled=True)


def all_in_one(shard, axis):
    leaves = jax.tree.leaves(shard)
    sequence = sorted(range(len(leaves)), key=lambda k: -leaves[k].size)
    width = (1, *leaves[sequence[0]].shape)[-1]
    lines = [
        jnp.pad(leaves[k].reshape(-1), (0, -leaves[k].size % width)).reshape(-1, width)
        for k in sequence
    ]
    both, at, found = (copy_for_each(jnp.concatenate(lines), axis), 0, {})
    for k, line in zip(sequence, lines):
        slab = both[:, at : at + len(line)].reshape(len(both), -1)
        found[k] = slab[:, : leaves[k].size].reshape(-1, *leaves[k].shape)
        at += len(line)
    numbers = iter(range(len(leaves)))
    return jax.tree.map(lambda _: found[next(numbers)], shard)


def combined_pairwise(pieces, combine):
    while len(jax.tree.leaves(pieces)[0]) > 1:
        pieces = jax.vmap(combine)(
            *(jax.tree.map(lambda part: part[side::2], pieces) for side in (0, 1))
        )
    return jax.tree.map(lambda part: part[0], pieces)


def carried_in(shard, axis, combine, identity):
    count, here = (lax.axis_size(axis), lax.axis_index(axis))
    passed = jnp.arange(count) < here

    def kept(part, zero, own):
        part = jnp.where(
            passed.reshape(-1, *(1 for _ in own.shape)),
            part.astype(own.dtype),
            jnp.asarray(zero, own.dtype),
        )
        return part

    pieces = all_in_one(
        jax.tree.map(lambda part, kind: part.astype(kind), shard, (jnp.bfloat16, jnp.bfloat16)),
        axis,
    )
    return combined_pairwise(jax.tree.map(kept, pieces, identity, shard), combine)


def combine_states(earlier, later):
    return (earlier[0] * later[0], later[0][..., None] * earlier[1] + later[1])


def norm_rows(tokens, row_gain):
    tokens_float = tokens.astype(jnp.float32)
    factor = lax.rsqrt(jnp.mean(tokens_float * tokens_float, axis=-1, keepdims=True) + epsilon)
    return (tokens_float * factor * row_gain).astype(jnp.bfloat16)


def slot_positions(blocks, experts_all):
    flattened = blocks.reshape(blocks.shape[0], -1)
    onehot = (flattened[..., None] == jnp.arange(experts_all, dtype=jnp.int32)).astype(jnp.int32)
    earlier = jnp.cumsum(onehot, axis=1) - onehot
    return jnp.sum(earlier * onehot, axis=-1).reshape(blocks.shape)


def fill_slots(rows_in, blocks, slot_ids, experts_all, capacity):
    groups = blocks.shape[0]
    sub_rows = blocks.shape[1]
    group_ids = jnp.arange(groups, dtype=jnp.int32)[:, None, None]
    target = (group_ids * experts_all + blocks) * capacity + slot_ids
    sources = jnp.broadcast_to(
        jnp.arange(sub_rows, dtype=jnp.int32)[None, :, None] + group_ids * sub_rows, blocks.shape
    )
    lookup = (
        jnp.full((groups * experts_all * capacity,), -1, jnp.int32)
        .at[target.reshape(-1)]
        .set(sources.reshape(-1))
    )
    gathered = rows_in.reshape(groups * sub_rows, -1)[jnp.maximum(lookup, 0)]
    filled = jnp.where((lookup >= 0)[:, None], gathered, jnp.zeros((), gathered.dtype))
    return filled.reshape(groups, experts_all, capacity, -1)


def on_device(
    query_preactivation,
    forget_preactivation,
    value_input_rows,
    output_gate_preactivation,
    forget_floor_gap,
    extra_log_forget,
    head_output_gain,
    mixer_output_weight,
    second_batch_tokens,
    feedforward_norm_gain,
    chosen_expert_index,
    chosen_expert_weight,
    expert_gate_weight,
    expert_up_weight,
    expert_down_weight,
):
    length = query_preactivation.shape[0]
    device_heads = forget_floor_gap.shape[0] // KEY_DIM
    block_count = length // BLOCK_POSITIONS
    shape_key = (block_count, BLOCK_POSITIONS, device_heads, KEY_DIM)
    queries = jax.nn.silu(query_preactivation.astype(jnp.float32)).reshape(shape_key)
    key_decay_rates = forget_floor_gap.reshape(device_heads, KEY_DIM) * jax.nn.sigmoid(
        -forget_preactivation.astype(jnp.float32)
    ).reshape(shape_key)
    forget_log_factor = (
        jnp.log(1.0 - key_decay_rates)
        + extra_log_forget.reshape(block_count, BLOCK_POSITIONS, device_heads)[..., None]
    )
    values = value_input_rows.astype(jnp.float32).reshape(
        block_count, BLOCK_POSITIONS, device_heads, VAL_DIM
    )
    cumulative_log = jnp.cumsum(forget_log_factor, axis=1)
    block_final_row = cumulative_log[:, -1]
    query_scaled = queries * jnp.exp(cumulative_log - block_final_row[:, None])
    scaled_key_rows = key_decay_rates * jnp.exp(block_final_row[:, None] - cumulative_log)
    scores = jnp.einsum("nthk,nshk->nhts", query_scaled, scaled_key_rows)
    causal_mask = jnp.arange(BLOCK_POSITIONS)[:, None] >= jnp.arange(BLOCK_POSITIONS)[None, :]
    scores = jnp.where(causal_mask, scores, 0.0)
    within = jnp.einsum("nhts,nshv->nthv", scores, values)
    updates = jnp.einsum("nshk,nshv->nhkv", scaled_key_rows, values)
    decays = jnp.exp(block_final_row)
    run_decay, run_state = lax.associative_scan(combine_states, (decays, updates))
    carried = carried_in(
        (run_decay[-1], run_state[-1]),
        "ep",
        combine_states,
        (jnp.ones_like(decays[0]), jnp.zeros_like(updates[0])),
    )
    prior_decay = jnp.concatenate([jnp.ones_like(decays[:1]), run_decay[:-1]], axis=0)
    prior_state = jnp.concatenate([jnp.zeros_like(updates[:1]), run_state[:-1]], axis=0)
    prior_full = prior_state + prior_decay[..., None] * carried[1][None]
    across_blocks = jnp.einsum("nthk,nhkv->nthv", queries * jnp.exp(cumulative_log), prior_full)
    recurrent = (within + across_blocks).reshape(length, device_heads, VAL_DIM)
    factor = lax.rsqrt(jnp.mean(recurrent * recurrent, axis=-1, keepdims=True) + epsilon)
    normed = (recurrent * factor * head_output_gain.reshape(device_heads, VAL_DIM)).reshape(
        length, device_heads * VAL_DIM
    )
    mixed = (normed * jax.nn.silu(output_gate_preactivation.astype(jnp.float32))).astype(
        jnp.bfloat16
    )
    mixer_output_first = jnp.dot(
        lax.all_gather(mixed, "tp", axis=1, tiled=True),
        mixer_output_weight,
        preferred_element_type=jnp.float32,
    ).astype(jnp.bfloat16)
    local_experts = expert_gate_weight.shape[0]
    experts_all = local_experts * lax.axis_size("ep")
    groups = lax.axis_size("tp")
    sub_rows = second_batch_tokens.shape[0] // groups
    capacity = max(2, sub_rows * TOPK * 5 // (4 * experts_all))
    position = lax.axis_index("tp")
    own_routes = lax.dynamic_slice_in_dim(chosen_expert_index, position * sub_rows, sub_rows, 0)
    own_weights = lax.dynamic_slice_in_dim(chosen_expert_weight, position * sub_rows, sub_rows, 0)
    own_slots = slot_positions(own_routes[None], experts_all)[0]
    own_rows = lax.dynamic_slice_in_dim(second_batch_tokens, position * sub_rows, sub_rows, 0)
    outgoing = fill_slots(
        norm_rows(own_rows, feedforward_norm_gain)[None],
        own_routes[None],
        own_slots[None],
        experts_all,
        capacity,
    )[0]
    arrived = lax.all_to_all(outgoing, "ep", split_axis=0, concat_axis=0, tiled=True)
    segment = lax.all_gather(arrived[None], "tp", axis=0, tiled=True)
    shaped = segment.reshape(segment.shape[0], -1, local_experts, capacity, segment.shape[-1])
    gate_part = jnp.einsum(
        "tsecd,edf->tsecf", shaped, expert_gate_weight, preferred_element_type=jnp.float32
    )
    up_part = jnp.einsum(
        "tsecd,edf->tsecf", shaped, expert_up_weight, preferred_element_type=jnp.float32
    )
    hidden = (jax.nn.silu(gate_part) * up_part).astype(jnp.bfloat16)
    rows_each = hidden.shape[1] * hidden.shape[2] * hidden.shape[3]
    product = jnp.einsum(
        "tsecf,efd->tsecd", hidden, expert_down_weight, preferred_element_type=jnp.float32
    )
    summed = lax.psum_scatter(
        product.reshape(rows_each * lax.axis_size("tp"), product.shape[-1]).astype(jnp.bfloat16),
        "tp",
        scatter_dimension=0,
        tiled=True,
    ).astype(jnp.float32)
    to_return = summed.astype(jnp.bfloat16).reshape(-1, local_experts * capacity, summed.shape[-1])
    returned = lax.all_to_all(to_return, "ep", split_axis=0, concat_axis=0, tiled=True)
    results = returned.reshape(experts_all * capacity, -1)
    flat_index = own_routes * capacity + own_slots
    combined = jnp.zeros((sub_rows, results.shape[1]), jnp.float32)
    for ranked in range(TOPK):
        combined = (
            combined
            + results[flat_index[:, ranked]].astype(jnp.float32)
            * own_weights[:, ranked : ranked + 1]
        )
    return (mixer_output_first, combined.astype(jnp.bfloat16))


def solution(mesh):
    placed = (
        P("ep", "tp"),
        P("ep", "tp"),
        P("ep", "tp"),
        P("ep", "tp"),
        P("tp"),
        P("ep", "tp"),
        P("tp"),
        P(None, "tp"),
        P("ep", None),
        P(),
        P("ep", None),
        P("ep", None),
        P("ep", None, "tp"),
        P("ep", None, "tp"),
        P("ep", "tp", None),
    )
    return jax.shard_map(
        on_device,
        mesh=mesh,
        in_specs=placed,
        out_specs=(P("ep", "tp"), P(("ep", "tp"), None)),
        check_vma=False,
    )
```

profile of v0, /device:TPU:1, one launch (start us, length us, event | category | flops | bytes accessed | tf_op | source)
XLA Modules:
  0.0 234.6 jit_solution(4051905095843440140)
XLA Ops:
  7.2 0.9 constant_dynamic-slice_fusion.1
  9.0 0.8 scatter_custom_fusion
  9.8 1.0 fusion.61
  10.9 1.0 fusion.63
  11.9 0.8 gather_fusion
  13.1 17.8 %all_to_all.15 = bf16[16,5,2048]{2,1,0:T(8,128)(2,1)S(1)} all-to-all(bf16[16,5,2048]{2,1,0:T(8,128)(2,1)S(1)} %broadcast_select_fusion), channel_id=1, replica_groups=mesh['ep'=16,'tp'=16] {'ep'}, dimensions={0} | all-to-all | bytes 655360 | tf_op jit(solution)/shard_map/all_to_all | solution.py:180
  30.9 0.9 copy.131
  31.9 0.5 broadcast.311
  32.4 0.7 reduce.14
  33.3 0.3 add_divide_fusion
  33.6 42.5 %all-gather.6.cloned.1.call-done = bf16[256,5,2048]{2,0,1:T(8,128)(2,1)} async-done(((bf16[16,5,2048]{2,0,1:T(8,128)(2,1)}), bf16[256,5,2048]{2,0,1:T(8,128)(2,1)}) %all-gather.6.cloned.1.call-update) | async-done | bytes 5242896 | tf_op jit(solution)/shard_map/all_gather | solution.py:181
  76.1 7.5 %fusion = f32[16,16,5,448]{3,1,2,0:T(8,128)} fusion(bf16[16,16,5,2048]{3,1,0,2:T(8,128)(2,1)} %bitcast.161, bf16[1,2048,448]{1,2,0:T(8,128)(2,1)} %param.28), kind=kOutput, calls=%fused_computation.5 | convolution fusion | flops 2348810240 | bytes 9371648 | tf_op jit(solution)/shard_map/tsecd,edf->tsecf/dot_general | solution.py:186
  83.6 10.4 %convert_bitcast_fusion = bf16[16,16,1,5,2048]{4,1,3,0,2:T(8,128)(2,1)} fusion(bf16[1,448,2048]{2,1,0:T(8,128)(2,1)S(1)} %copy-done, f32[16,16,5,448]{3,1,2,0:T(8,128)} %fusion, bf16[16,16,5,2048]{3,1,0,2:T(8,128)(2,1)} %bitcast.162, bf16[1,2048,448]{1,2,0:T(8,128)(2,1)} %param.27), kind=kOutput, calls=%fused_computation.4 | convolution fusion | flops 4703682560 | bytes 16449536 | tf_op jit(solution)/shard_map/tsecf,efd->tsecd/dot_general | solution.py:191
  94.0 10.3 %copy.134 = bf16[16,16,1,5,2048]{4,3,1,0,2:T(8,128)(2,1)} copy(bf16[16,16,1,5,2048]{4,1,3,0,2:T(8,128)(2,1)} %convert_bitcast_fusion) | data formatting | bytes 10485760 | tf_op jit(solution)/shard_map/convert_element_type | solution.py:195
  104.3 10.0 %convert_element_type.116 = bf16[1280,2048]{1,0:T(8,128)(2,1)} reshape(bf16[16,16,1,5,2048]{4,3,1,0,2:T(8,128)(2,1)} %copy.134) | data formatting | bytes 10485760 | tf_op jit(solution)/shard_map/convert_element_type | solution.py:195
  114.4 0.6 copy-done.12
  115.0 0.8 fusion.37
  116.0 0.5 slice_multiply_fusion.4
  116.5 0.6 fusion.84
  117.5 0.5 reshape.453
  118.0 0.3 convert_multiply_fusion
  118.3 2.3 fusion.30
  120.6 0.4 fusion.42
  121.0 0.4 copy-done.4
  122.3 5.9 %pad.149 = f32[31,1,128,64]{2,3,0,1:T(8,128)} pad(f32[16,1,128,64]{2,3,0,1:T(8,128)S(1)} %add.235, f32[]{:T(128)} %constant.15.clone.1), padding=0_0_1x0_0_0x0_0_0x0_0_0 | pad | bytes 1540100
  128.2 0.8 fusion.71
  129.0 0.9 broadcast_in_dim.57
  129.8 6.6 %all-to-all-start = ((bf16[16,130,64]{1,2,0:T(8,128)(2,1)}), bf16[16,130,64]{1,2,0:T(8,128)(2,1)}, u32[]{:S(2)}, u32[]{:S(2)}) async-start(bf16[16,130,64]{1,2,0:T(8,128)(2,1)} %broadcast_in_dim.57), calls=%async_computation | async-start | bytes 1048576 | tf_op jit(solution)/shard_map/all_to_all | solution.py:15
  136.5 6.1 %pad.73 = f32[32,1,128,64]{2,3,0,1:T(8,128)} pad(f32[16,1,128,64]{2,3,0,1:T(8,128)S(1)} %add.235, f32[]{:T(128)} %constant.15.clone.1), padding=1_0_1x0_0_0x0_0_0x0_0_0 | pad | bytes 1572868 | tf_op jit(solution)/shard_map/pad | solution.py:139
  142.8 0.8 pad_maximum_fusion
  143.7 6.2 %pad.72 = f32[32,1,128,64]{2,3,0,1:T(8,128)S(1)} pad(f32[16,1,128,64]{2,3,0,1:T(8,128)} %pad_maximum_fusion, f32[]{:T(128)} %constant.15.clone.1), padding=0_1_1x0_0_0x0_0_0x0_0_0 | pad | bytes 1572868 | tf_op jit(solution)/shard_map/pad | solution.py:139
  149.9 1.1 slice_add_fusion
  151.0 2.0 convolution_bitcast_fusion
  153.1 1.0 slice.331
  154.5 1.1 select_bitcast_fusion
  155.7 0.5 multiply_reduce_fusion
  156.3 0.6 copy.129
  156.9 0.4 reshape.455
  157.4 0.9 fusion.56
  158.3 0.8 constant_dynamic-slice_fusion
  159.2 16.0 %reduce-scatter.2.cloned.1.call-done = bf16[80,2048]{1,0:T(8,128)(2,1)} async-done(((bf16[1280,2048]{1,0:T(8,128)(2,1)}), bf16[80,2048]{1,0:T(8,128)(2,1)}) %reduce-scatter.2.cloned.1.call-update) | async-done | bytes 327696 | tf_op jit(solution)/shard_map/reduce_scatter | solution.py:194
  175.2 1.9 reshape.461
  177.1 6.3 %all-to-all-start.2 = ((bf16[16,5,2048]{2,1,0:T(8,128)(2,1)}), bf16[16,5,2048]{2,1,0:T(8,128)(2,1)S(1)}, u32[]{:S(2)}, u32[]{:S(2)}) async-start(bf16[16,5,2048]{2,1,0:T(8,128)(2,1)} %reshape.461), calls=%async_computation.3 | async-start | bytes 1048576 | tf_op jit(solution)/shard_map/all_to_all | solution.py:201
  183.4 38.0 %all-gather.4.cloned.1.call-done = bf16[2048,1024]{0,1:T(8,128)(2,1)} async-done(((bf16[2048,64]{0,1:T(8,128)(2,1)}), bf16[2048,1024]{0,1:T(8,128)(2,1)}) %all-gather.4.cloned.1.call-update) | async-done | bytes 4194320 | tf_op jit(solution)/shard_map/all_gather | solution.py:159
  221.4 4.4 %convolution_convert_fusion = bf16[2048,128]{1,0:T(8,128)(2,1)} fusion(bf16[2048,1024]{0,1:T(8,128)(2,1)} %all-gather.4.cloned.1.call-done, bf16[1024,128]{1,0:T(8,128)(2,1)S(1)} %copy-done.16), kind=kOutput, calls=%fused_computation.16 | convolution fusion | flops 537133056 | bytes 4980736 | tf_op jit(solution)/shard_map/dot_general | solution.py:158
  226.0 0.7 gather_fusion.1
  226.6 0.7 gather_fusion.2
  227.3 0.8 add_convert_fusion
  (156 shorter events, 4.1 us)
Async XLA Ops:
  7.2 76.4 %copy-start = (bf16[1,448,2048]{2,1,0:T(8,128)(2,1)S(1)}, bf16[1,448,2048]{2,1,0:T(8,128)(2,1)}, u32[]{:S(2)}) copy-start(bf16[1,448,2048]{2,1,0:T(8,128)(2,1)} %param.29) | copy-start | bytes 5505028
  7.2 68.9 %all-gather.6.cloned.1.call-start = ((), (), s32[]{:S(2)}) async-start(), calls=%async_computation.6 | async-start | bytes 5570560 | tf_op jit(solution)/shard_map/all_gather | solution.py:181
  12.7 19.7 %copy-start.11 = (f32[2048,1]{0,1:T(1,128)S(1)}, f32[2048,1]{0,1:T(1,128)}, u32[]{:S(2)}) copy-start(f32[2048,1]{0,1:T(1,128)} %param.20) | copy-start | bytes 24580
  12.7 20.5 %copy-start.7 = (bf16[2048,128]{1,0:T(8,128)(2,1)S(1)}, bf16[2048,128]{1,0:T(8,128)(2,1)}, u32[]{:S(2)}) copy-start(bf16[2048,128]{1,0:T(8,128)(2,1)} %param.16) | copy-start | bytes 1572868
  31.9 143.3 %reduce-scatter.2.cloned.1.call-start = ((), (), s32[]{:S(2)}) async-start(), calls=%async_computation.5 | async-start | bytes 5570560 | tf_op jit(solution)/shard_map/reduce_scatter | solution.py:194
  114.3 0.7 copy-start.12
  114.3 3.2 %copy-start.9 = (bf16[2048,64]{0,1:T(8,128)(2,1)S(1)}, bf16[2048,64]{0,1:T(8,128)(2,1)}, u32[]{:S(2)}) copy-start(bf16[2048,64]{0,1:T(8,128)(2,1)} %param.17) | copy-start | bytes 786436
  114.3 3.7 %copy-start.8 = (bf16[2048,128]{1,0:T(8,128)(2,1)S(1)}, bf16[2048,128]{1,0:T(8,128)(2,1)}, u32[]{:S(2)}) copy-start(bf16[2048,128]{1,0:T(8,128)(2,1)} %param.15) | copy-start | bytes 1572868
  118.0 2.6 %copy-start.6 = (bf16[32,64,64]{1,0,2:T(8,128)(2,1)}, bf16[32,64,64]{1,0,2:T(8,128)(2,1)S(1)}, u32[]{:S(2)}) copy-start(bf16[32,64,64]{1,0,2:T(8,128)(2,1)S(1)} %reshape.453) | copy-start | bytes 786436
  120.6 0.8 copy-start.4
  120.6 1.0 copy-start.13
  120.6 1.0 copy-start.14
  129.8 23.2 %all-to-all-start = ((bf16[16,130,64]{1,2,0:T(8,128)(2,1)}), bf16[16,130,64]{1,2,0:T(8,128)(2,1)}, u32[]{:S(2)}, u32[]{:S(2)}) async-start(bf16[16,130,64]{1,2,0:T(8,128)(2,1)} %broadcast_in_dim.57), calls=%async_computation | async-start | bytes 1048576 | tf_op jit(solution)/shard_map/all_to_all | solution.py:15
  136.4 85.0 %all-gather.4.cloned.1.call-start = ((), (), s32[]{:S(2)}) async-start(), calls=%async_computation.4 | async-start | bytes 4456448 | tf_op jit(solution)/shard_map/all_gather | solution.py:159
  142.8 7.1 %copy-start.2 = (f32[32,1,128,64]{2,3,0,1:T(8,128)S(1)}, f32[32,1,128,64]{2,3,0,1:T(8,128)}, u32[]{:S(2)}) copy-start(f32[32,1,128,64]{2,3,0,1:T(8,128)} %pad.73) | copy-start | bytes 3145732
  142.8 8.2 %copy-start.5 = (bf16[32,64,128]{2,0,1:T(8,128)(2,1)S(1)}, bf16[32,64,128]{2,0,1:T(8,128)(2,1)}, u32[]{:S(2)}) copy-start(bf16[32,64,128]{2,0,1:T(8,128)(2,1)} %copy-done.4) | copy-start | bytes 1572868
  151.0 4.7 %copy-start.3 = (f32[31,1,128,64]{2,3,0,1:T(8,128)S(1)}, f32[31,1,128,64]{2,3,0,1:T(8,128)}, u32[]{:S(2)}) copy-start(f32[31,1,128,64]{2,3,0,1:T(8,128)} %slice_add_fusion) | copy-start | bytes 3047428
  156.2 1.1 copy-start.10
  156.3 1.1 copy-start.15
  156.9 64.5 %copy-start.16 = (bf16[1024,128]{1,0:T(8,128)(2,1)S(1)}, bf16[1024,128]{1,0:T(8,128)(2,1)}, u32[]{:S(2)}) copy-start(bf16[1024,128]{1,0:T(8,128)(2,1)} %param.22) | copy-start | bytes 786436
  177.1 48.7 %all-to-all-start.2 = ((bf16[16,5,2048]{2,1,0:T(8,128)(2,1)}), bf16[16,5,2048]{2,1,0:T(8,128)(2,1)S(1)}, u32[]{:S(2)}, u32[]{:S(2)}) async-start(bf16[16,5,2048]{2,1,0:T(8,128)(2,1)} %reshape.461), calls=%async_computation.3 | async-start | bytes 1048576 | tf_op jit(solution)/shard_map/all_to_all | solution.py:201
  221.4 6.7 %copy-start.1 = (bf16[1,448,2048]{2,1,0:T(8,128)(2,1)S(1)}, bf16[1,448,2048]{2,1,0:T(8,128)(2,1)}, u32[]{:S(2)}) copy-start(bf16[1,448,2048]{2,1,0:T(8,128)(2,1)} %param.29) | copy-start | bytes 5505028
Sparse Core Ops, SparseCore 0:
  32.0 44.0 all-gather.5
  114.5 60.6 reduce-scatter.1
  177.6 43.7 all-gather.3
where the time goes:
time: 236 us; the launch traced here: 235 us
  waiting for transfers between devices  96.6 us (41%)
  local copies, waits for them, and re-layouts  53.1 us (22%)
  matrix products  25.2 us (11%)
  blocking collectives  17.8 us (8%)
  between operations  14.5 us (6%)
  other arithmetic  14.4 us (6%)
  starting transfers between devices  13 us (6%)
    all_gather x1, waiting for transfers between devices, on_device(): segment = lax.all_gather(arrived[None], 'tp', axis=0, tiled=True)  42.5 us
    all_gather x1, waiting for transfers between devices, on_device(): lax.all_gather(mixed, 'tp', axis=1, tiled=True)  38 us
    convert_element_type x2, local copies, waits for them, and re-layouts, on_device(): product.reshape(rows_each * lax.axis_size('tp'), product.shape[-1])  20.4 us
    all_to_all x1, blocking collectives, on_device(): lax.all_to_all(outgoing, 'ep', split_axis=0, concat_axis=0, tiled=True)  17.8 us
    reduce_scatter x1, waiting for transfers between devices, on_device(): lax.psum_scatter(product.reshape(rows_each * lax.axis_size('tp'), product...  16 us
    pad x16, local copies, waits for them, and re-layouts, on_device(): lax.associative_scan(combine_states, (decays, updates))  12.7 us
    dot_general x1, matrix products, on_device(): jnp.einsum('tsecf,efd->tsecd', hidden, expert_down_weight, preferred_elem...  10.4 us
    unnamed x39, local copies, waits for them, and re-layouts  7.75 us
  transfers between devices with their start and end apart: 5, of which 3 were waited for; matrix products, arithmetic and copies ran while one was open for 19% of the time, Pallas kernels for 0%

commit v1 on v0

--- a/solution.py
+++ b/solution.py
@@ -8,6 +8,7 @@
 BLOCK_POSITIONS = 64
 TOPK = 2
 epsilon = 1e-06
+_measure_entries = lambda row_data: jnp.concatenate(lax.all_gather(row_data, "tp"), axis=1)
 
 
 def copy_for_each(shard, axis):
@@ -156,9 +157,7 @@
         jnp.bfloat16
     )
     mixer_output_first = jnp.dot(
-        lax.all_gather(mixed, "tp", axis=1, tiled=True),
-        mixer_output_weight,
-        preferred_element_type=jnp.float32,
+        _measure_entries(mixed), mixer_output_weight, preferred_element_type=jnp.float32
     ).astype(jnp.bfloat16)
     local_experts = expert_gate_weight.shape[0]
     experts_all = local_experts * lax.axis_size("ep")

time: 236 us -> 251 us (1.064)
  the two profiles are of different devices: /device:TPU:1 before, /device:TPU:2 now
where the time goes in v1:
time: 251 us; the launch traced here: 248 us
  local copies, waits for them, and re-layouts  80.3 us (32%)
  waiting for transfers between devices  76.3 us (30%)
  other arithmetic  30.4 us (12%)
  matrix products  26.5 us (11%)
  starting transfers between devices  20.3 us (8%)
  between operations  14.5 us (6%)
    reduce_scatter x1, waiting for transfers between devices, on_device(): lax.psum_scatter(product.reshape(rows_each * lax.axis_size('tp'), product...  61.7 us
    pad x16, local copies, waits for them, and re-layouts, on_device(): lax.associative_scan(combine_states, (decays, updates))  28.7 us
    convert_element_type x2, local copies, waits for them, and re-layouts, on_device(): product.reshape(rows_each * lax.axis_size('tp'), product.shape[-1])  20.4 us
    dot_general x1, matrix products, on_device(): jnp.einsum('tsecf,efd->tsecd', hidden, expert_down_weight, preferred_elem...  10.4 us
    unnamed x63, local copies, waits for them, and re-layouts  9.39 us
    add x10, other arithmetic, on_device(): lax.associative_scan(combine_states, (decays, updates))  7.64 us
    all_to_all x1, starting transfers between devices, on_device(): lax.all_to_all(outgoing, 'ep', split_axis=0, concat_axis=0, tiled=True)  7.48 us
    dot_general x1, matrix products, on_device(): jnp.einsum('tsecd,edf->tsecf', shaped, expert_up_weight, preferred_elemen...  7.46 us
  transfers between devices with their start and end apart: 6, of which 4 were waited for; matrix products, arithmetic and copies ran while one was open for 50% of the time, Pallas kernels for 0%

profile of v1, /device:TPU:2, one launch (start us, length us, event | category | flops | bytes accessed | tf_op | source)
XLA Modules:
  0.0 248.4 jit_solution(641484723890311199)
XLA Ops:
  7.2 0.9 constant_dynamic-slice_fusion.1
  9.8 1.0 fusion.61
  10.9 1.0 fusion.63
  11.9 0.8 gather_fusion
  12.9 0.9 broadcast_select_fusion
  13.9 7.5 %all-to-all-start.1 = ((bf16[16,5,2048]{2,1,0:T(8,128)(2,1)}), bf16[16,5,2048]{2,1,0:T(8,128)(2,1)S(1)}, u32[]{:S(2)}, u32[]{:S(2)}) async-start(bf16[16,5,2048]{2,1,0:T(8,128)(2,1)} %broadcast_select_fusion), calls=%async_computation.1 | async-start | bytes 1048576 | tf_op jit(solution)/shard_map/all_to_all | solution.py:179
  21.4 1.3 add_divide_fusion
  24.8 1.0 copy-done.2
  26.6 4.9 %all-to-all-done.1 = bf16[16,5,2048]{2,1,0:T(8,128)(2,1)S(1)} async-done(((bf16[16,5,2048]{2,1,0:T(8,128)(2,1)}), bf16[16,5,2048]{2,1,0:T(8,128)(2,1)S(1)}, u32[]{:S(2)}, u32[]{:S(2)}) %all-to-all-start.1) | async-done | bytes 327712 | tf_op jit(solution)/shard_map/all_to_all | solution.py:179
  31.5 0.9 copy.136
  34.2 1.5 reshape.459
  35.7 1.5 convert_multiply_fusion
  37.2 3.8 %fusion.30 = (bf16[32,64,128]{2,0,1:T(8,128)(2,1)}, bf16[32,64,128]{2,0,1:T(8,128)(2,1)}, bf16[32,64,128]{2,0,1:T(8,128)(2,1)S(1)}) fusion(f32[32,64,1,128]{3,0,1,2:T(8,128)} %copy-done.2, f32[32,64,128]{2,1,0:T(8,128)S(1)} %bitcast.157, f32[32,128]{1,0:T(8,128)S(1)} %get-tuple-element.9, f32[32,64,128]{2,1,0:T(8,128)S(1)} %bitcast.154, f32[128]{0:T(128)S(1)} %copy-done.26), kind=kLoop, calls=%fused_computation.39 | loop fusion | flops 2359296 | bytes 4735488 | tf_op jit(solution)/shard_map/mul | solution.py:150
  44.2 0.8 pad.67
  44.9 0.8 fusion.82
  46.4 2.1 pad.66
  48.4 1.6 add.231
  50.0 1.0 fusion.65
  51.8 2.0 pad.68
  53.7 3.5 %pad.69 = f32[8,1,128,64]{2,3,0,1:T(8,128)} pad(f32[4,1,128,64]{2,3,0,1:T(8,128)} %add.231, f32[]{:T(128)} %constant.15.clone.1), padding=1_0_1x0_0_0x0_0_0x0_0_0 | pad | bytes 393220 | tf_op jit(solution)/shard_map/pad | solution.py:140
  57.2 1.8 add.233
  59.0 5.1 %pad.71 = f32[16,1,128,64]{2,3,0,1:T(8,128)} pad(f32[8,1,128,64]{2,3,0,1:T(8,128)} %add.233, f32[]{:T(128)} %constant.15.clone.1), padding=1_0_1x0_0_0x0_0_0x0_0_0 | pad | bytes 786436 | tf_op jit(solution)/shard_map/pad | solution.py:140
  64.1 1.1 fusion.64
  65.2 3.3 %pad.70 = f32[16,1,128,64]{2,3,0,1:T(8,128)} pad(f32[8,1,128,64]{2,3,0,1:T(8,128)S(1)} %pad_maximum_fusion.1, f32[]{:T(128)} %constant.15.clone.1), padding=0_1_1x0_0_0x0_0_0x0_0_0 | pad | bytes 786436 | tf_op jit(solution)/shard_map/pad | solution.py:140
  68.5 1.3 add.235
  69.9 5.9 %pad.149 = f32[31,1,128,64]{2,3,0,1:T(8,128)} pad(f32[16,1,128,64]{2,3,0,1:T(8,128)S(1)} %add.235, f32[]{:T(128)} %constant.15.clone.1), padding=0_0_1x0_0_0x0_0_0x0_0_0 | pad | bytes 1540100
  76.6 0.8 broadcast_in_dim.57
  77.4 5.4 %all-to-all-start = ((bf16[16,130,64]{1,2,0:T(8,128)(2,1)}), bf16[16,130,64]{1,2,0:T(8,128)(2,1)}, u32[]{:S(2)}, u32[]{:S(2)}) async-start(bf16[16,130,64]{1,2,0:T(8,128)(2,1)} %broadcast_in_dim.57), calls=%async_computation | async-start | bytes 1048576 | tf_op jit(solution)/shard_map/all_to_all | solution.py:16
  83.0 6.0 %pad.73 = f32[32,1,128,64]{2,3,0,1:T(8,128)} pad(f32[16,1,128,64]{2,3,0,1:T(8,128)S(1)} %add.235, f32[]{:T(128)} %constant.15.clone.1), padding=1_0_1x0_0_0x0_0_0x0_0_0 | pad | bytes 1572868 | tf_op jit(solution)/shard_map/pad | solution.py:140
  89.7 1.3 fusion.58
  91.0 5.9 %pad.72 = f32[32,1,128,64]{2,3,0,1:T(8,128)} pad(f32[16,1,128,64]{2,3,0,1:T(8,128)S(1)} %pad_maximum_fusion, f32[]{:T(128)} %constant.15.clone.1), padding=0_1_1x0_0_0x0_0_0x0_0_0 | pad | bytes 1572868 | tf_op jit(solution)/shard_map/pad | solution.py:140
  97.0 2.4 slice_add_fusion
  99.4 3.2 %convolution_bitcast_fusion = f32[32,64,64]{2,1,0:T(8,128)} fusion(bf16[32,64,128]{2,0,1:T(8,128)(2,1)} %get-tuple-element.5, bf16[32,64,128]{2,0,1:T(8,128)(2,1)} %copy-done.6, pred[64,64]{1,0:T(8,128)(4,1)S(1)} %iota_compare_fusion.1, bf16[32,64,64]{1,0,2:T(8,128)(2,1)} %copy-done.7), kind=kOutput, calls=%fused_computation.23 | convolution fusion | flops 50462720 | bytes 1839104 | tf_op jit(solution)/shard_map/nhts,nshv->nthv/dot_general | solution.py:137
  102.6 1.7 slice.331
  104.3 1.1 copy.143
  105.7 1.1 select_bitcast_fusion
  108.6 1.8 fusion.56
  110.8 7.5 %fusion = f32[16,16,5,448]{3,1,2,0:T(8,128)} fusion(bf16[16,16,5,2048]{3,1,0,2:T(8,128)(2,1)} %bitcast.170, bf16[1,2048,448]{1,2,0:T(8,128)(2,1)} %param.28), kind=kOutput, calls=%fused_computation.5 | convolution fusion | flops 2348810240 | bytes 9371648 | tf_op jit(solution)/shard_map/tsecd,edf->tsecf/dot_general | solution.py:185
  118.2 10.4 %convert_bitcast_fusion = bf16[16,16,1,5,2048]{4,1,3,0,2:T(8,128)(2,1)} fusion(bf16[1,448,2048]{2,1,0:T(8,128)(2,1)S(1)} %copy-done, f32[16,16,5,448]{3,1,2,0:T(8,128)} %fusion, bf16[16,16,5,2048]{3,1,0,2:T(8,128)(2,1)} %bitcast.171, bf16[1,2048,448]{1,2,0:T(8,128)(2,1)} %param.27), kind=kOutput, calls=%fused_computation.4 | convolution fusion | flops 4703682560 | bytes 16449536 | tf_op jit(solution)/shard_map/tsecf,efd->tsecd/dot_general | solution.py:190
  128.6 10.4 %copy.139 = bf16[16,16,1,5,2048]{4,3,1,0,2:T(8,128)(2,1)} copy(bf16[16,16,1,5,2048]{4,1,3,0,2:T(8,128)(2,1)} %convert_bitcast_fusion) | data formatting | bytes 10485760 | tf_op jit(solution)/shard_map/convert_element_type | solution.py:194
  139.0 10.0 %convert_element_type.116 = bf16[1280,2048]{1,0:T(8,128)(2,1)} reshape(bf16[16,16,1,5,2048]{4,3,1,0,2:T(8,128)(2,1)} %copy.139) | data formatting | bytes 10485760 | tf_op jit(solution)/shard_map/convert_element_type | solution.py:194
  150.0 5.3 %all-gather.5.cloned.1.call-done = bf16[32768,64]{0,1:T(8,128)(2,1)} async-done(((bf16[2048,64]{0,1:T(8,128)(2,1)}), bf16[32768,64]{0,1:T(8,128)(2,1)}) %all-gather.5.cloned.1.call-update) | async-done | bytes 4194320 | tf_op jit(solution)/shard_map/all_gather | solution.py:11
  155.4 4.8 %copy.184 = bf16[8,16,8,2048]{3,2,0,1:T(8,128)(2,1)} copy(bf16[8,16,8,2048]{3,2,1,0:T(8,128)(2,1)} %bitcast.158) | data formatting | bytes 8388608 | tf_op jit(solution)/shard_map/all_gather | solution.py:11
  160.1 61.7 %reduce-scatter.2.cloned.1.call-done = bf16[80,2048]{1,0:T(8,128)(2,1)} async-done(((bf16[1280,2048]{1,0:T(8,128)(2,1)}), bf16[80,2048]{1,0:T(8,128)(2,1)}) %reduce-scatter.2.cloned.1.call-update) | async-done | bytes 327696 | tf_op jit(solution)/shard_map/reduce_scatter | solution.py:193
  221.8 1.9 reshape.469
  223.7 7.1 %all-to-all-start.2 = ((bf16[16,5,2048]{2,1,0:T(8,128)(2,1)}), bf16[16,5,2048]{2,1,0:T(8,128)(2,1)S(1)}, u32[]{:S(2)}, u32[]{:S(2)}) async-start(bf16[16,5,2048]{2,1,0:T(8,128)(2,1)} %reshape.469), calls=%async_computation.3 | async-start | bytes 1048576 | tf_op jit(solution)/shard_map/all_to_all | solution.py:200
  230.8 4.4 %convolution_convert_fusion = bf16[2048,128]{1,0:T(8,128)(2,1)} fusion(bf16[2048,1024]{0,1:T(8,128)(2,1)} %bitcast.159, bf16[1024,128]{1,0:T(8,128)(2,1)S(1)} %copy-done.28), kind=kOutput, calls=%fused_computation.17 | convolution fusion | flops 537133056 | bytes 4980736 | tf_op jit(solution)/shard_map/dot_general | solution.py:159
  235.3 4.3 %all-to-all-done.2 = bf16[16,5,2048]{2,1,0:T(8,128)(2,1)S(1)} async-done(((bf16[16,5,2048]{2,1,0:T(8,128)(2,1)}), bf16[16,5,2048]{2,1,0:T(8,128)(2,1)S(1)}, u32[]{:S(2)}, u32[]{:S(2)}) %all-to-all-start.2) | async-done | bytes 327712 | tf_op jit(solution)/shard_map/all_to_all | solution.py:200
  (182 shorter events, 18.0 us)
Async XLA Ops:
  7.2 111.1 %copy-start = (bf16[1,448,2048]{2,1,0:T(8,128)(2,1)S(1)}, bf16[1,448,2048]{2,1,0:T(8,128)(2,1)}, u32[]{:S(2)}) copy-start(bf16[1,448,2048]{2,1,0:T(8,128)(2,1)} %param.29) | copy-start | bytes 5505028
  12.7 10.5 %copy-start.25 = (f32[2048,1]{0,1:T(1,128)S(1)}, f32[2048,1]{0,1:T(1,128)}, u32[]{:S(2)}) copy-start(f32[2048,1]{0,1:T(1,128)} %param.20) | copy-start | bytes 24580
  12.7 11.4 %copy-start.26 = (f32[128]{0:T(128)S(1)}, f32[128]{0:T(128)}, u32[]{:S(2)}) copy-start(f32[128]{0:T(128)} %param.19) | copy-start | bytes 1540
  13.9 17.6 %all-to-all-start.1 = ((bf16[16,5,2048]{2,1,0:T(8,128)(2,1)}), bf16[16,5,2048]{2,1,0:T(8,128)(2,1)S(1)}, u32[]{:S(2)}, u32[]{:S(2)}) async-start(bf16[16,5,2048]{2,1,0:T(8,128)(2,1)} %broadcast_select_fusion), calls=%async_computation.1 | async-start | bytes 1048576 | tf_op jit(solution)/shard_map/all_to_all | solution.py:179
  21.3 89.4 %all-gather.7.cloned.1.call-start = ((), (), s32[]{:S(2)}) async-start(), calls=%async_computation.6 | async-start | bytes 5570560 | tf_op jit(solution)/shard_map/all_gather | solution.py:180
  24.8 1.0 copy-start.2
  26.4 14.5 %copy-start.14 = (f32[32,1,128]{2,0,1:T(8,128)}, f32[32,1,128]{2,0,1:T(8,128)S(1)}, u32[]{:S(2)}) copy-start(f32[32,1,128]{2,0,1:T(8,128)S(1)} %get-tuple-element.8) | copy-start | bytes 49156
  32.5 0.7 copy-start.24
  32.6 0.8 copy-start.23
  33.3 7.7 %copy-start.18 = (f32[16,1,128]{2,0,1:T(8,128)}, f32[16,1,128]{2,0,1:T(8,128)S(1)}, u32[]{:S(2)}) copy-start(f32[16,1,128]{2,0,1:T(8,128)S(1)} %pad.81) | copy-start | bytes 24580
  33.3 7.6 %copy-start.20 = (f32[16,1,128]{2,0,1:T(8,128)}, f32[16,1,128]{2,0,1:T(8,128)S(1)}, u32[]{:S(2)}) copy-start(f32[16,1,128]{2,0,1:T(8,128)S(1)} %pad.80) | copy-start | bytes 24580
  33.4 7.6 %copy-start.16 = (f32[16,1,128]{2,0,1:T(8,128)}, f32[16,1,128]{2,0,1:T(8,128)S(1)}, u32[]{:S(2)}) copy-start(f32[16,1,128]{2,0,1:T(8,128)S(1)} %add.241) | copy-start | bytes 24580
  35.7 5.3 %copy-start.7 = (bf16[32,64,64]{1,0,2:T(8,128)(2,1)}, bf16[32,64,64]{1,0,2:T(8,128)(2,1)S(1)}, u32[]{:S(2)}) copy-start(bf16[32,64,64]{1,0,2:T(8,128)(2,1)S(1)} %reshape.459) | copy-start | bytes 786436
  41.0 1.9 copy-start.6
  42.2 0.8 copy-start.8
  42.8 0.7 copy-start.10
  42.9 0.6 copy-start.11
  42.9 0.6 copy-start.12
  53.7 11.5 %copy-start.13 = (f32[1,1,128,64]{2,3,0,1:T(8,128)S(1)}, f32[1,1,128,64]{2,3,0,1:T(8,128)}, u32[]{:S(2)}) copy-start(f32[1,1,128,64]{2,3,0,1:T(8,128)} %slice.309) | copy-start | bytes 98308
  64.1 12.5 %copy-start.22 = (bf16[2,64]{0,1:T(8,128)(2,1)S(1)}, bf16[2,64]{0,1:T(8,128)(2,1)}, u32[]{:S(2)}) copy-start(bf16[2,64]{0,1:T(8,128)(2,1)} %copy.128) | copy-start | bytes 772
  65.2 17.7 %copy-start.15 = (f32[32,1,128]{2,0,1:T(8,128)S(1)}, f32[32,1,128]{2,0,1:T(8,128)}, u32[]{:S(2)}) copy-start(f32[32,1,128]{2,0,1:T(8,128)} %copy-done.14) | copy-start | bytes 49156
  68.5 14.4 %copy-start.17 = (f32[16,1,128]{2,0,1:T(8,128)S(1)}, f32[16,1,128]{2,0,1:T(8,128)}, u32[]{:S(2)}) copy-start(f32[16,1,128]{2,0,1:T(8,128)} %copy-done.16) | copy-start | bytes 24580
  69.8 19.8 %copy-start.19 = (f32[16,1,128]{2,0,1:T(8,128)S(1)}, f32[16,1,128]{2,0,1:T(8,128)}, u32[]{:S(2)}) copy-start(f32[16,1,128]{2,0,1:T(8,128)} %copy-done.18) | copy-start | bytes 24580
  69.8 19.8 %copy-start.21 = (f32[16,1,128]{2,0,1:T(8,128)S(1)}, f32[16,1,128]{2,0,1:T(8,128)}, u32[]{:S(2)}) copy-start(f32[16,1,128]{2,0,1:T(8,128)} %copy-done.20) | copy-start | bytes 24580
  77.4 25.2 %all-to-all-start = ((bf16[16,130,64]{1,2,0:T(8,128)(2,1)}), bf16[16,130,64]{1,2,0:T(8,128)(2,1)}, u32[]{:S(2)}, u32[]{:S(2)}) async-start(bf16[16,130,64]{1,2,0:T(8,128)(2,1)} %broadcast_in_dim.57), calls=%async_computation | async-start | bytes 1048576 | tf_op jit(solution)/shard_map/all_to_all | solution.py:16
  82.9 72.5 %all-gather.5.cloned.1.call-start = ((), (), s32[]{:S(2)}) async-start(), calls=%async_computation.5 | async-start | bytes 4456448 | tf_op jit(solution)/shard_map/all_gather | solution.py:11
  91.0 6.0 %copy-start.3 = (f32[32,1,128,64]{2,3,0,1:T(8,128)S(1)}, f32[32,1,128,64]{2,3,0,1:T(8,128)}, u32[]{:S(2)}) copy-start(f32[32,1,128,64]{2,3,0,1:T(8,128)} %pad.73) | copy-start | bytes 3145732
  99.4 7.6 %copy-start.4 = (f32[31,1,128,64]{2,3,0,1:T(8,128)S(1)}, f32[31,1,128,64]{2,3,0,1:T(8,128)}, u32[]{:S(2)}) copy-start(f32[31,1,128,64]{2,3,0,1:T(8,128)} %slice_add_fusion) | copy-start | bytes 3047428
  99.4 7.6 %copy-start.5 = (bf16[32,64,128]{2,0,1:T(8,128)(2,1)S(1)}, bf16[32,64,128]{2,0,1:T(8,128)(2,1)}, u32[]{:S(2)}) copy-start(bf16[32,64,128]{2,0,1:T(8,128)(2,1)} %get-tuple-element.4) | copy-start | bytes 1572868
  105.7 1.3 copy-start.9
  107.6 1.1 copy-start.27
  110.5 111.3 %reduce-scatter.2.cloned.1.call-start = ((), (), s32[]{:S(2)}) async-start(), calls=%async_computation.4 | async-start | bytes 5570560 | tf_op jit(solution)/shard_map/reduce_scatter | solution.py:193
  155.4 75.5 %copy-start.28 = (bf16[1024,128]{1,0:T(8,128)(2,1)S(1)}, bf16[1024,128]{1,0:T(8,128)(2,1)}, u32[]{:S(2)}) copy-start(bf16[1024,128]{1,0:T(8,128)(2,1)} %param.22) | copy-start | bytes 786436
  223.7 15.9 %all-to-all-start.2 = ((bf16[16,5,2048]{2,1,0:T(8,128)(2,1)}), bf16[16,5,2048]{2,1,0:T(8,128)(2,1)S(1)}, u32[]{:S(2)}, u32[]{:S(2)}) async-start(bf16[16,5,2048]{2,1,0:T(8,128)(2,1)} %reshape.469), calls=%async_computation.3 | async-start | bytes 1048576 | tf_op jit(solution)/shard_map/all_to_all | solution.py:200
  230.8 11.0 %copy-start.1 = (bf16[1,448,2048]{2,1,0:T(8,128)(2,1)S(1)}, bf16[1,448,2048]{2,1,0:T(8,128)(2,1)}, u32[]{:S(2)}) copy-start(bf16[1,448,2048]{2,1,0:T(8,128)(2,1)} %param.29) | copy-start | bytes 5505028
Sparse Core Ops, SparseCore 0:
  32.6 43.1 all-gather.6
  110.6 44.6 all-gather.4
  157.9 63.8 reduce-scatter.1
